TPU v7x, 32 devices: a whole 2x2x4 slice. The times are simulated.
32 devices in a mesh: sp: 8 (over z, y), tp: 4 (over x, core).
Axes of the slice: x: 2, y: 2, z: 4, core: 2. Of those that a mesh axis runs over, the one named last changes fastest.
Arguments:
- tokens: bfloat16 [1024, 2048], P('sp', 'tp'), may hold values from -28 to 28
- norm_gain: bfloat16 [1, 2048], P(None, 'tp'), may hold values from 0.099609375 to 1.8984375
- conv_b_w: bfloat16 [2048, 1024], P(None, 'tp'), may hold values from -0.125 to 0.125
- conv_c_w: bfloat16 [2048, 1024], P(None, 'tp'), may hold values from -0.125 to 0.125
- conv_u_w: bfloat16 [2048, 1024], P(None, 'tp'), may hold values from -0.125 to 0.125
- conv_taps: bfloat16 [3, 1024], P(None, 'tp'), may hold values from -3.5 to 3.5
- query_w: bfloat16 [2048, 2048], P(None, 'tp'), may hold values from -0.125 to 0.125
- key_w: bfloat16 [2048, 2048], P(None, 'tp'), may hold values from -0.125 to 0.125
- value_w: bfloat16 [2048, 2048], P(None, 'tp'), may hold values from -0.125 to 0.125
- outgate_w: bfloat16 [2048, 2048], P(None, 'tp'), may hold values from -0.125 to 0.125
- gate_w: bfloat16 [2048, 2, 8], P(None, None, 'tp'), may hold values from -0.125 to 0.125
- gate_bias: float32 [2, 8], P(None, 'tp'), may hold values from -5 to 150
- mem_gain: bfloat16 [2048], P('tp'), may hold values from 0.099609375 to 1.8984375
- conv_out_w: bfloat16 [1024, 2048], P('tp'), may hold values from -0.1875 to 0.1875
- mem_out_w: bfloat16 [2048, 2048], P('tp'), may hold values from -0.125 to 0.125
Outputs:
- layer_out: bfloat16 [1024, 2048], P(('sp', 'tp'))
All inputs are finite; a program needn't handle non-finite values.
Results may differ from a plain program's by a relative error of at most 0.014.
The roundings to bfloat16 on the way count: a program that leaves them out, or rounds other values in their place, can miss the bound.
Values may be sent and summed in bfloat16 or wider, within the bound.
A program may use at most 64 MiB of HBM per device.

v0:
```python
import jax
import jax.numpy as jnp
from jax import lax
from jax.sharding import PartitionSpec as P

HEAD_DIM = 256
BLOCK = 128
MDIM = 2048


EPS = 1e-06
LOWEST = -1e30
HIGH = lax.Precision.HIGHEST


def shifted(value, axis, by):
    count = lax.axis_size(axis)
    pairs = [(i, i + by) for i in range(count) if 0 <= i + by < count]
    return lax.ppermute(value, axis, pairs)


def prefix(value, axis, join, neutral):
    count, mine = (lax.axis_size(axis), lax.axis_index(axis))
    pieces = jax.tree.map(lambda part: lax.all_gather(part, axis), value)
    total = jax.tree.map(
        lambda part, zero: jnp.full_like(part, 0) + jnp.asarray(zero, part.dtype), value, neutral
    )

    def prefix_step(position, total):
        longer = join(total, jax.tree.map(lambda part: part[position], pieces))
        return jax.tree.map(lambda new, old: jnp.where(position < mine, new, old), longer, total)

    return lax.fori_loop(0, count - 1, prefix_step, total)


def local_pass(queries, keys, values, input_pre, log_forget):
    count, width = queries.shape
    blocks = count // BLOCK

    def local_step(carry, inputs):
        memory, normer, stabil, decay_sum = carry
        query_block, key_block, value_block, input_gate, forget_block = inputs
        causal = jnp.tril(jnp.ones((BLOCK, BLOCK), dtype=bool))
        running = jnp.cumsum(forget_block)
        decays = jnp.where(
            causal, running[:, None] - running[None, :] + input_gate[None, :], -jnp.inf
        )
        inter = running + stabil
        row_max = jnp.maximum(inter, jnp.max(decays, axis=1))
        weights = jnp.exp(decays - row_max[:, None])
        scores = jnp.dot(query_block, key_block.T, precision=HIGH) * weights
        carried = jnp.exp(inter - row_max)
        numer_part = carried[:, None] * jnp.dot(query_block, memory, precision=HIGH) + jnp.dot(
            scores, value_block, precision=HIGH
        )
        denom_part = carried * jnp.dot(query_block, normer, precision=HIGH) + jnp.sum(
            scores, axis=1
        )
        new_stabil = row_max[-1]
        key_weight = jnp.exp(running[-1] - running + input_gate - new_stabil)
        fade = jnp.exp(running[-1] + stabil - new_stabil)
        memory = fade * memory + jnp.dot(
            (key_weight[:, None] * key_block).T, value_block, precision=HIGH
        )
        normer = fade * normer + jnp.dot(key_weight, key_block, precision=HIGH)
        outputs = (numer_part, denom_part, row_max, decay_sum + running)
        return ((memory, normer, new_stabil, decay_sum + running[-1]), outputs)

    inputs = (
        queries.reshape(blocks, BLOCK, width),
        keys.reshape(blocks, BLOCK, width),
        values.reshape(blocks, BLOCK, width),
        input_pre.reshape(blocks, BLOCK),
        log_forget.reshape(blocks, BLOCK),
    )
    start = (
        jnp.zeros((width, width), jnp.float32),
        jnp.zeros((width,), jnp.float32),
        jnp.zeros((), jnp.float32),
        jnp.zeros((), jnp.float32),
    )
    final, rows = lax.scan(local_step, start, inputs)
    memory, normer, stabil, decay_sum = final
    numer_rows, denom_rows, row_max, row_decay = rows
    return (
        numer_rows.reshape(count, width),
        denom_rows.reshape(count),
        row_max.reshape(count),
        row_decay.reshape(count),
        decay_sum,
        stabil,
        memory,
        normer,
    )


def finish(queries, numer_rows, denom_rows, row_max, row_decay, stabil_in, memory_in, normer_in):
    from_before = jnp.dot(queries, memory_in, precision=HIGH)
    normer_before = jnp.dot(queries, normer_in, precision=HIGH)
    top = jnp.maximum(row_max, row_decay + stabil_in)
    own_scale = jnp.exp(row_max - top)
    past_scale = jnp.exp(row_decay + stabil_in - top)
    numer_all = own_scale[:, None] * numer_rows + past_scale[:, None] * from_before
    denom_all = own_scale * denom_rows + past_scale * normer_before
    return numer_all / jnp.maximum(jnp.abs(denom_all), jnp.exp(-top))[:, None]


def join_state(earlier, later):
    sum_early, stab_early, mem_early, norm_early = earlier[:4]
    sum_late, stab_late, mem_late, norm_late = later[:4]
    top = jnp.maximum(sum_late + stab_early, stab_late)
    early_scale = jnp.exp(sum_late + stab_early - top)
    late_scale = jnp.exp(stab_late - top)
    joined = (
        sum_early + sum_late,
        top,
        early_scale[:, None, None] * mem_early + late_scale[:, None, None] * mem_late,
        early_scale[:, None] * norm_early + late_scale[:, None] * norm_late,
    )
    if len(earlier) > 4:
        edge = jnp.where(later[5][0] > 0, later[4], earlier[4])
        joined = joined + (edge, jnp.maximum(earlier[5], later[5]))
    return joined


def body(
    tokens,
    norm_gain,
    conv_b_w,
    conv_c_w,
    conv_u_w,
    conv_taps,
    query_w,
    key_w,
    value_w,
    outgate_w,
    gate_w,
    gate_bias,
    mem_gain,
    conv_out_w,
    mem_out_w,
):
    count = tokens.shape[0]
    model = conv_b_w.shape[0]
    weights = (
        conv_b_w,
        conv_c_w,
        conv_u_w,
        query_w,
        key_w,
        value_w,
        outgate_w,
        gate_w.reshape(model, -1),
    )
    piece = lax.all_gather(tokens, "tp", axis=1, tiled=True)
    gain_piece = lax.all_gather(norm_gain, "tp", axis=1, tiled=True)
    wide = piece.astype(jnp.float32)
    scaled = (wide * gain_piece.astype(jnp.float32)).astype(jnp.bfloat16)
    squares = jnp.sum(wide * wide, axis=1)
    totals = tuple(
        (jnp.dot(scaled, weight, preferred_element_type=jnp.float32) for weight in weights)
    )
    folded = (squares,) + totals
    inv_rms = lax.rsqrt(folded[0] / model + EPS)[:, None]

    def project(total):
        return lax.optimization_barrier((inv_rms * total).astype(jnp.bfloat16)).astype(jnp.float32)

    gate_b, gate_c, gate_u, queries, keys, values, outgate = [
        project(total) for total in folded[1:8]
    ]
    heads = gate_bias.shape[1]
    gates = inv_rms * folded[8]
    input_pre = gates[:, :heads] + gate_bias[0]
    forget_pre = gates[:, heads:] + gate_bias[1]
    mixed_in = (gate_c * gate_u).astype(jnp.bfloat16)
    reach = conv_taps.shape[0] - 1
    head_q = queries.reshape(count, heads, HEAD_DIM)
    head_k = keys.reshape(count, heads, HEAD_DIM) * HEAD_DIM ** (-0.5)
    head_v = values.reshape(count, heads, HEAD_DIM)
    local = jax.vmap(local_pass, in_axes=1, out_axes=(1, 1, 1, 1, 0, 0, 0, 0))(
        head_q, head_k, head_v, input_pre, jax.nn.log_sigmoid(forget_pre)
    )
    numer_rows, denom_rows, row_max, row_decay, decay_sum, stabil, memory, normer = local
    identity = (
        jnp.zeros((heads,), jnp.float32),
        jnp.full((heads,), LOWEST, jnp.float32),
        jnp.zeros((heads, HEAD_DIM, HEAD_DIM), jnp.float32),
        jnp.zeros((heads, HEAD_DIM), jnp.float32),
    )
    before = shifted(mixed_in[count - reach :], "sp", 1)
    incoming = prefix((decay_sum, stabil, memory, normer), "sp", join_state, identity)
    padded = jnp.concatenate([before, mixed_in], axis=0).astype(jnp.float32)
    taps = conv_taps.astype(jnp.float32)
    conv_sum = taps[0] * padded[0:count]
    for offset in range(1, reach + 1):
        conv_sum = conv_sum + taps[offset] * padded[offset : offset + count]
    y_conv = (gate_b * conv_sum).astype(jnp.bfloat16)
    mem_raw = jax.vmap(finish, in_axes=(1, 1, 1, 1, 1, 0, 0, 0), out_axes=1)(
        head_q, numer_rows, denom_rows, row_max, row_decay, incoming[1], incoming[2], incoming[3]
    )
    flat_raw = mem_raw.reshape(count, -1)
    own_squares = jnp.sum(flat_raw * flat_raw, axis=1)
    all_squares = lax.psum(own_squares, "tp")
    mem_norm = flat_raw * lax.rsqrt(all_squares / MDIM + EPS)[:, None]
    mem_norm = mem_norm * mem_gain.astype(jnp.float32)[None, :]
    y_mem = (jax.nn.sigmoid(outgate) * mem_norm).astype(jnp.bfloat16)
    return lax.psum_scatter(
        (
            jnp.dot(y_conv, conv_out_w, preferred_element_type=jnp.float32)
            + jnp.dot(y_mem, mem_out_w, preferred_element_type=jnp.float32)
        ).astype(jnp.bfloat16),
        "tp",
        scatter_dimension=0,
        tiled=True,
    )


def solution(mesh):
    return jax.shard_map(
        body,
        mesh=mesh,
        in_specs=(
            P("sp", "tp"),
            P(None, "tp"),
            P(None, "tp"),
            P(None, "tp"),
            P(None, "tp"),
            P(None, "tp"),
            P(None, "tp"),
            P(None, "tp"),
            P(None, "tp"),
            P(None, "tp"),
            P(None, None, "tp"),
            P(None, "tp"),
            P("tp"),
            P("tp", None),
            P("tp", None),
        ),
        out_specs=P(("sp", "tp"), None),
        check_vma=False,
    )
```

profile of v0, /device:TPU:25, one launch (start us, length us, event | category | flops | bytes accessed | tf_op | source)
XLA Modules:
  0.0 147.0 jit_solution(2480114630991469454)
XLA Ops:
  6.6 0.8 slice_bitcast_fusion
  7.4 5.8 %all_gather.31 = bf16[1,2048]{1,0:T(2,128)(2,1)S(1)} all-gather(bf16[1,512]{1,0:T(2,128)(2,1)} %param.18), channel_id=1, replica_groups=mesh['sp'=8,'tp'=4] {'tp'}, dimensions={1}, use_global_device_ids=true | all-gather | bytes 5120 | tf_op jit(solution)/shard_map/all_gather | solution.py:156
  13.2 0.7 reshape.140
  14.0 7.5 %all_gather.30 = bf16[128,2048]{1,0:T(8,128)(2,1)S(1)} all-gather(bf16[128,512]{1,0:T(8,128)(2,1)} %param.17), channel_id=1, replica_groups=mesh['sp'=8,'tp'=4] {'tp'}, dimensions={1}, use_global_device_ids=true | all-gather | bytes 655360 | tf_op jit(solution)/shard_map/all_gather | solution.py:155
  21.5 0.2 fusion.21
  21.7 0.2 convolution_multiply_fusion.8
  21.9 0.1 add_bitcast_fusion
  22.0 0.3 reduce_window_sum.14
  22.3 0.1 fusion.41
  22.5 0.2 multiply_reduce_fusion.1
  22.7 0.1 subtract_exponential_fusion.4
  22.8 2.2 %fusion.15 = bf16[128,512]{1,0:T(8,128)(2,1)S(1)} fusion(bf16[2048,512]{1,0:T(8,128)(2,1)} %param.24, f32[128]{0:T(128)S(1)} %add_rsqrt_fusion.1, bf16[128,2048]{1,0:T(8,128)(2,1)S(1)} %all_gather.30, f32[2048]{0:T(1024)S(1)} %bitcast.213), kind=kOutput, calls=%fused_computation.34 | convolution fusion | flops 269352960 | bytes 2761216 | tf_op jit(solution)/shard_map/dot_general | solution.py:161
  25.0 0.4 fusion.16
  25.5 1.3 convolution_add_fusion.1
  26.8 0.0 all-gather.7.cloned.1.call-update
  26.8 0.0 reduce-scatter.2.cloned.1.call-start
  26.9 1.5 %fusion.19 = bf16[128,256]{1,0:T(8,128)(2,1)S(1)} fusion(bf16[2048,256]{1,0:T(8,128)(2,1)} %param.20, f32[128]{0:T(128)S(1)} %add_rsqrt_fusion.1, bf16[128,2048]{1,0:T(8,128)(2,1)S(1)} %all_gather.30, f32[2048]{0:T(1024)S(1)} %bitcast.215), kind=kOutput, calls=%fused_computation.42 | convolution fusion | flops 135069696 | bytes 1647104 | tf_op jit(solution)/shard_map/dot_general | solution.py:161
  28.4 0.0 copy-start.4
  28.4 1.5 %fusion.20 = bf16[128,256]{1,0:T(8,128)(2,1)S(1)} fusion(bf16[2048,256]{1,0:T(8,128)(2,1)} %param.21, f32[128]{0:T(128)S(1)} %add_rsqrt_fusion.1, bf16[128,2048]{1,0:T(8,128)(2,1)S(1)} %all_gather.30, f32[2048]{0:T(1024)S(1)} %bitcast.216), kind=kOutput, calls=%fused_computation.43 | convolution fusion | flops 135069696 | bytes 1647104 | tf_op jit(solution)/shard_map/dot_general | solution.py:161
  30.0 3.1 %collective-permute-start = (bf16[2,256]{1,0:T(2,128)(2,1)S(1)}, bf16[2,256]{1,0:T(2,128)(2,1)S(1)}, u32[]{:S(2)}, u32[]{:S(2)}) collective-permute-start(bf16[2,256]{1,0:T(2,128)(2,1)S(1)} %slice.57), channel_id=1, source_target_pairs={{0,4},{4,8},{8,12},{12,16},{16,20},{20,24},{24,28},{1,5},{5,9},{9,... | collective-permute-start | bytes 3080 | tf_op jit(solution)/shard_map/ppermute | solution.py:19
  33.2 0.6 dynamic-slice.10
  34.4 0.2 dynamic-update-slice
  34.7 0.2 dynamic-update-slice.1
  34.9 2.3 %fusion.17 = bf16[128,512]{1,0:T(8,128)(2,1)S(1)} fusion(bf16[2048,512]{1,0:T(8,128)(2,1)} %param.23, f32[128]{0:T(128)S(1)} %add_rsqrt_fusion.1, bf16[128,2048]{1,0:T(8,128)(2,1)S(1)} %all_gather.30, f32[2048]{0:T(1024)S(1)} %bitcast.217), kind=kOutput, calls=%fused_computation.36 | convolution fusion | flops 269352960 | bytes 2761216 | tf_op jit(solution)/shard_map/dot_general | solution.py:161
  37.2 0.0 copy-start.2
  37.2 0.2 fusion.23
  37.4 0.1 fusion.63
  37.5 0.2 fusion.33
  37.7 0.3 fusion.80
  38.0 0.3 convolution_bitcast_fusion.2
  38.4 0.0 copy-start.5
  38.4 0.3 fusion.18
  38.7 0.1 copy-done.2
  38.8 0.4 fusion.14
  39.2 19.2 %all-gather.4 = f32[8,2,256]{2,1,0:T(2,128)S(1)} all-gather(f32[1,2,256]{2,1,0:T(2,128)S(1)} %fusion.63), channel_id=5, replica_groups=mesh['sp'=8,'tp'=4] {'sp'}, dimensions={0}, use_global_device_ids=true | all-gather | bytes 18432 | tf_op jit(solution)/shard_map/all_gather | solution.py:24
  58.5 16.8 %all-reduce.2 = (f32[16]{0:T(128)S(1)}, f32[16]{0:T(128)S(1)}) all-reduce(f32[16]{0:T(128)S(1)} %dynamic-update-slice, f32[16]{0:T(128)S(1)} %dynamic-update-slice.1), channel_id=2, replica_groups=mesh['sp'=8,'tp'=4] {'sp'}, use_global_device_ids=true, to_apply=%add | all-reduce | flops 32 | bytes 256
  75.4 0.1 reshape.145
  75.4 0.1 reshape.146
  75.5 0.0 collective-permute-done
  75.6 2.6 %fusion.50 = f32[128,2048]{1,0:T(8,128)} fusion(bf16[256,2048]{1,0:T(8,128)(2,1)} %param.30, f32[130,256]{1,0:T(8,128)S(1)} %maximum_convert_fusion, bf16[128,256]{1,0:T(8,128)(2,1)S(1)} %fusion.18, f32[256]{0:T(256)S(1)} %bitcast.230, f32[256]{0:T(256)S(1)} %bitcast.229, f32[256]{0:T(256)S(1)} %bitcast.228), kind=kOutput, calls=%fused_computation.85 | convolution fusion | flops 134479872 | bytes 2558976 | tf_op jit(solution)/shard_map/dot_general | solution.py:210
  78.1 21.4 %all-gather.7.cloned.1.call-done = f32[16,256,256]{2,1,0:T(8,128)} async-done(((f32[2,256,256]{2,1,0:T(8,128)}), f32[16,256,256]{2,1,0:T(8,128)}) %all-gather.7.cloned.1.call-update) | async-done | bytes 4194320 | tf_op jit(solution)/shard_map/all_gather | solution.py:24
  99.5 9.3 %while.5 = (s32[]{:T(128)}, f32[2]{0:T(128)S(1)}, f32[2,256,256]{2,1,0:T(8,128)S(1)}, f32[2,256]{1,0:T(2,128)S(1)}, s32[]{:T(128)}, /*index=5*/f32[8,2]{1,0:T(8,...) while((s32[]{:T(128)}, f32[2]{0:T(128)S(1)}, ...), condition=%wide.region_4.5_spmd.clone, body=%wide.region_3.4_spmd.clone.sunk | while | flops 657940 | bytes 1579278 | solution.py:33
  99.6 0.1 fusion.97
  99.7 1.2 fusion.96
  100.9 0.1 fusion.97
  101.0 1.2 fusion.96
  102.3 0.1 fusion.97
  102.3 1.2 fusion.96
  103.6 0.1 fusion.97
  103.7 1.2 fusion.96
  104.9 0.1 fusion.97
  105.0 1.2 fusion.96
  106.3 0.1 fusion.97
  106.4 1.2 fusion.96
  107.6 0.1 fusion.97
  107.7 1.2 fusion.96
  108.9 0.2 fusion.31
  109.1 0.1 fusion.71
  109.1 0.3 fusion.13
  109.4 0.5 multiply_reduce_fusion
  109.9 5.7 %psum.7 = f32[128]{0:T(128)S(1)} all-reduce(f32[128]{0:T(128)S(1)} %get-tuple-element.276), channel_id=1, replica_groups=mesh['sp'=8,'tp'=4] {'tp'}, use_global_device_ids=true, to_apply=%region_7.8 | all-reduce | flops 128 | bytes 1024 | tf_op jit(solution)/shard_map/psum | solution.py:204
  115.7 2.5 %fusion.7 = bf16[128,2048]{1,0:T(8,128)(2,1)} fusion(f32[128,2048]{1,0:T(8,128)} %fusion.50, bf16[512,2048]{1,0:T(8,128)(2,1)S(1)} %copy-done, f32[128,512]{1,0:T(8,128)S(1)} %bitcast.211, bf16[128,512]{1,0:T(8,128)(2,1)S(1)} %fusion.14, f32[512]{0:T(512)S(1)} %convert_element_type.84, f32[128]{0:T(128)S(1)} %add_rsqrt_fusion), kind=kOutput, calls=%fused_computation.16 | convolution fusion | flops 269484032 | bytes 4065792 | tf_op jit(solution)/shard_map/dot_general | solution.py:211
  118.2 0.0 reduce-scatter.2.cloned.1.call-update
  118.2 21.9 %reduce-scatter.2.cloned.1.call-done = bf16[32,2048]{1,0:T(8,128)(2,1)} async-done(((bf16[128,2048]{1,0:T(8,128)(2,1)}), bf16[32,2048]{1,0:T(8,128)(2,1)}) %reduce-scatter.2.cloned.1.call-update) | async-done | bytes 131088 | tf_op jit(solution)/shard_map/reduce_scatter | solution.py:208
  (43 shorter events, 0.4 us)
Async XLA Ops:
  6.5 109.2 %copy-start = (bf16[512,2048]{1,0:T(8,128)(2,1)S(1)}, bf16[512,2048]{1,0:T(8,128)(2,1)}, u32[]{:S(2)}) copy-start(bf16[512,2048]{1,0:T(8,128)(2,1)} %param.31) | copy-start | bytes 6291460
  6.5 93.0 %all-gather.7.cloned.1.call-start = ((), (), s32[]{:S(2)}) async-start(), calls=%async_computation.2 | async-start | bytes 4718592 | tf_op jit(solution)/shard_map/all_gather | solution.py:24
  22.3 2.7 %copy-start.1 = (bf16[2048,512]{1,0:T(8,128)(2,1)S(1)}, bf16[2048,512]{1,0:T(8,128)(2,1)}, u32[]{:S(2)}) copy-start(bf16[2048,512]{1,0:T(8,128)(2,1)} %param.25) | copy-start | bytes 6291460
  26.8 6.4 %copy-start.6 = (u32[32]{0:T(128)S(1)}, u32[32]{0:T(128)}, u32[]{:S(2)}) copy-start(u32[32]{0:T(128)} %constant.86) | copy-start | bytes 388
  26.8 113.4 %reduce-scatter.2.cloned.1.call-start = ((), (), s32[]{:S(2)}) async-start(), calls=%async_computation.1 | async-start | bytes 655360 | tf_op jit(solution)/shard_map/reduce_scatter | solution.py:208
  28.4 9.1 %copy-start.4 = (bf16[3,256]{1,0:T(4,128)(2,1)S(1)}, bf16[3,256]{1,0:T(4,128)(2,1)}, u32[]{:S(2)}) copy-start(bf16[3,256]{1,0:T(4,128)(2,1)} %param.22) | copy-start | bytes 4612
  30.0 45.5 %collective-permute-start = (bf16[2,256]{1,0:T(2,128)(2,1)S(1)}, bf16[2,256]{1,0:T(2,128)(2,1)S(1)}, u32[]{:S(2)}, u32[]{:S(2)}) collective-permute-start(bf16[2,256]{1,0:T(2,128)(2,1)S(1)} %slice.57), channel_id=1, source_target_pairs={{0,4},{4,8},{8,12},{12,16},{16,20},{20,24},{24,28},{1,5},{5,9},{9,... | collective-permute-start | bytes 3080 | tf_op jit(solution)/shard_map/ppermute | solution.py:19
  34.9 3.5 %copy-start.3 = (bf16[2048,256]{1,0:T(8,128)(2,1)S(1)}, bf16[2048,256]{1,0:T(8,128)(2,1)}, u32[]{:S(2)}) copy-start(bf16[2048,256]{1,0:T(8,128)(2,1)} %param.19) | copy-start | bytes 3145732
  37.2 1.6 %copy-start.2 = (bf16[2048,512]{1,0:T(8,128)(2,1)S(1)}, bf16[2048,512]{1,0:T(8,128)(2,1)}, u32[]{:S(2)}) copy-start(bf16[2048,512]{1,0:T(8,128)(2,1)} %param.26) | copy-start | bytes 6291460
  38.4 37.0 %copy-start.5 = (bf16[512]{0:T(512)(128)(2,1)S(1)}, bf16[512]{0:T(512)(128)(2,1)}, u32[]{:S(2)}) copy-start(bf16[512]{0:T(512)(128)(2,1)} %param.29) | copy-start | bytes 3076
Sparse Core Ops, SparseCore 0:
  26.9 72.5 all-gather.6
  118.4 21.7 reduce-scatter.1
where the time goes:
time: 150 us; the launch traced here: 147 us
  blocking collectives  55.1 us (37%)
  waiting for transfers between devices  43.4 us (29%)
  matrix products  17.4 us (12%)
  between operations  14.3 us (10%)
  other arithmetic  10.4 us (7%)
  starting transfers between devices  3.19 us (2%)
  local copies, waits for them, and re-layouts  2.92 us (2%)
    reduce_scatter x1, waiting for transfers between devices, body(): lax.psum_scatter((jnp.dot(y_conv, conv_out_w, preferred_element_type=jnp....  21.9 us
    all_gather x1, waiting for transfers between devices, prefix(): pieces = jax.tree.map(lambda part: lax.all_gather(part, axis), value)  21.4 us
    all_gather x1, blocking collectives, prefix(): pieces = jax.tree.map(lambda part: lax.all_gather(part, axis), value)  19.2 us
    unnamed x1, blocking collectives  16.8 us
    dot_general x8, matrix products, body(): jnp.dot(scaled, weight, preferred_element_type=jnp.float32)  9.01 us
    select_n x14, other arithmetic, prefix_step(): jnp.where(position < mine, new, old)  8.88 us
    all_gather x1, blocking collectives, body(): piece = lax.all_gather(tokens, 'tp', axis=1, tiled=True)  7.49 us
    all_gather x1, blocking collectives, body(): gain_piece = lax.all_gather(norm_gain, 'tp', axis=1, tiled=True)  5.82 us
  transfers between devices with their start and end apart: 3, of which 2 were waited for; matrix products, arithmetic and copies ran while one was open for 8% of the time, Pallas kernels for 0%

commit v1 on v0

v1 whole, which is shorter than its diff:
```python
import functools

import jax
import jax.numpy as jnp
from jax import lax
from jax.experimental import pallas as pl
from jax.experimental.pallas import tpu as pltpu
from jax.sharding import PartitionSpec as P

EPS = 1e-06
LOWEST = -1e30
HIGH = lax.Precision.HIGHEST
MESH = pl.DeviceIdType.MESH
F32 = jnp.float32
BF16 = jnp.bfloat16
GROUP = 128
NCHUNK = 4
NOUT = 4
EXTRA = 16


def dot(a, b, dims=((1,), (0,)), precision=None):
    return lax.dot_general(a, b, (dims, ((), ())), precision=precision, preferred_element_type=F32)


def kernel(n_sp, n_tp, heads, *refs):
    (tok, gain, wb, wc, wu, taps, wq, wk, wv, wo, gw, bias, mgain, cow, mow, out) = refs[:16]
    (
        full, scaled, vb, vc, vu, vq, vk, vv, vo, vg, vco, vmo,
        qs, ks, vs, og, own_c, got_a, got_p, put_p, in_c,
        meta, meta_a, meta_p, meta_s, meta_i, gates, gates_t,
        num, den, gb, mixed, halo, pad, yc, ym, sq_own, sq_got, part, rs,
        sem_w, sem_tok, tok_s, tok_r, a_s, a_r, p_s, p_r, h_s, h_r, q_s, q_r, r_s, r_r,
    ) = refs[16:]
    sp, tp = lax.axis_index("sp"), lax.axis_index("tp")
    count, feats = tok.shape
    model = n_tp * feats
    head_dim = wq.shape[1] // heads
    rows = head_dim // NCHUNK
    chips = n_tp // 2
    chip, core = tp // 2, lax.rem(tp, 2)
    mate = chip * 2 + 1 - core
    pair, odd = sp // 2, lax.rem(sp, 2)
    last_pair = n_sp // 2 - 1
    twin = sp + 1 - 2 * odd
    others = [lax.rem(tp + k, n_tp) for k in range(1, n_tp)]

    tok_copy = pltpu.make_async_copy(tok, full.at[tp, pl.ds(0, count)], sem_tok)
    tok_copy.start()
    loads = [
        pltpu.make_async_copy(src, dst, sem_w.at[i])
        for i, (src, dst) in enumerate(
            ((gw, vg), (wk, vk), (wv, vv), (wq, vq), (wc, vc), (wu, vu), (wb, vb), (wo, vo), (cow, vco), (mow, vmo))
        )
    ]
    for load in loads:
        load.start()
    wait_of = dict(zip(("g", "k", "v", "q", "c", "u", "b", "o", "co", "mo"), loads))
    full[tp, pl.ds(count, EXTRA), :] = jnp.broadcast_to(gain[...].astype(F32), (EXTRA, feats)).astype(BF16)

    barrier = pltpu.get_barrier_semaphore()
    steps = (1, -1, 2, -2)
    for other in others:
        pl.semaphore_signal(barrier, inc=1, device_id=(sp, other), device_id_type=MESH)
    for step in steps:
        @pl.when((sp + step >= 0) & (sp + step < n_sp))
        def _():
            pl.semaphore_signal(barrier, inc=1, device_id=(sp + step, tp), device_id_type=MESH)
    peers = n_tp - 1
    for step in steps:
        peers = peers + ((sp + step >= 0) & (sp + step < n_sp)).astype(jnp.int32)
    pl.semaphore_wait(barrier, peers)

    def send_tok(source, to, slot):
        copy = pltpu.make_async_remote_copy(
            src_ref=full.at[source], dst_ref=full.at[source], send_sem=tok_s.at[slot],
            recv_sem=tok_r.at[source], device_id=(sp, to), device_id_type=MESH)
        copy.start()
        return copy

    def got_tok(source):
        pltpu.make_async_remote_copy(
            src_ref=full.at[source], dst_ref=full.at[source], send_sem=tok_s.at[0],
            recv_sem=tok_r.at[source], device_id=(sp, mate), device_id_type=MESH).wait_recv()

    tok_copy.wait()
    tok_sends = []
    far = [lax.rem(chip + k, chips) for k in range(1, chips)]
    for k, x in enumerate(far):
        tok_sends.append(send_tok(tp, x * 2 + core, k))
    tok_sends.append(send_tok(tp, mate, chips - 1))
    for k, x in enumerate(far):
        got_tok(x * 2 + core)
        tok_sends.append(send_tok(x * 2 + core, mate, chips + k))
    got_tok(mate)
    for k, x in enumerate(far):
        got_tok(x * 2 + 1 - core)

    squares = jnp.zeros((count, 1), F32)
    for s in range(n_tp):
        wide = full[s, 0:count, :].astype(F32)
        scaled[:, s * feats:(s + 1) * feats] = (wide * full[s, count:count + 1, :].astype(F32)).astype(BF16)
        squares = squares + jnp.sum(wide * wide, axis=1, keepdims=True)
    inv = lax.rsqrt(squares / model + EPS)

    def project(ref, lo, hi):
        return (inv * dot(scaled[...], ref[:, lo:hi])).astype(BF16)

    wait_of["g"].wait()
    pre = inv * dot(scaled[...], vg[...], ((1,), (1,))) + bias[0:1, :]
    lf = jnp.minimum(pre, 0.0) - jnp.log1p(jnp.exp(-jnp.abs(pre)))
    row_id = lax.broadcasted_iota(jnp.int32, (count, count), 0)
    col_id = lax.broadcasted_iota(jnp.int32, (count, count), 1)
    causal = row_id >= col_id
    running = dot(causal.astype(F32), lf, precision=HIGH)
    lane = lax.broadcasted_iota(jnp.int32, (count, GROUP), 1)
    both = jnp.where(lane < heads, pre, running)
    gates[...] = both
    gates_t[...] = both.T

    def gate_parts(h):
        i_col, b_col = gates[:, h:h + 1], gates[:, heads + h:heads + h + 1]
        i_row, b_row = gates_t[h:h + 1, :], gates_t[heads + h:heads + h + 1, :]
        decays = jnp.where(causal, b_col - b_row + i_row, LOWEST)
        top = jnp.max(decays, axis=1, keepdims=True)
        return i_col, b_col, decays, top

    wait_of["k"].wait()
    wait_of["v"].wait()
    scale = head_dim ** -0.5
    a_sends = []

    def remote(src, dst, ss, rs_, to):
        return pltpu.make_async_remote_copy(
            src_ref=src, dst_ref=dst, send_sem=ss, recv_sem=rs_, device_id=to, device_id_type=MESH)

    for h in range(heads):
        lo, hi = h * head_dim, (h + 1) * head_dim
        ks[:, lo:hi] = project(vk, lo, hi)
        vs[:, lo:hi] = project(vv, lo, hi)
        i_col, b_col, _, top = gate_parts(h)
        total = b_col[count - 1:count, :]
        m_own = top[count - 1:count, :]
        weight = jnp.exp(total - b_col + i_col - m_own)
        wkeys = ks[:, lo:hi].astype(F32) * (weight * scale)
        meta[h, 0:1, :] = jnp.sum(wkeys, axis=0, keepdims=True)
        meta[h, 1:2, :] = jnp.broadcast_to(m_own, (1, head_dim))
        meta[h, 2:3, :] = jnp.broadcast_to(total, (1, head_dim))
        meta[h, 3:8, :] = jnp.zeros((5, head_dim), F32)
        own_c[h] = dot(wkeys.astype(BF16), vs[:, lo:hi], ((0,), (0,))).astype(BF16)
        copy = remote(meta.at[h], meta_a.at[h], a_s.at[h, NCHUNK], a_r.at[h, NCHUNK], (twin, tp))
        copy.start()
        a_sends.append(copy)
        for c in range(NCHUNK):
            at = pl.ds(c * rows, rows)
            copy = remote(own_c.at[h, at], got_a.at[h, at], a_s.at[h, c], a_r.at[h, c], (twin, tp))
            copy.start()
            a_sends.append(copy)

    wait_of["c"].wait()
    wait_of["u"].wait()
    conv = wc.shape[1]
    mix = (project(vc, 0, conv).astype(F32) * project(vu, 0, conv).astype(F32)).astype(BF16)
    mixed[...] = mix
    edge = remote(mixed.at[pl.ds(count - EXTRA, EXTRA)], halo, h_s, h_r, (sp + 1, tp))
    pl.when(sp < n_sp - 1)(edge.start)
    wait_of["q"].wait()
    for h in range(heads):
        qs[:, h * head_dim:(h + 1) * head_dim] = project(vq, h * head_dim, (h + 1) * head_dim)
    wait_of["b"].wait()
    gb[...] = project(vb, 0, conv)
    wait_of["o"].wait()
    for h in range(heads):
        og[:, h * head_dim:(h + 1) * head_dim] = project(vo, h * head_dim, (h + 1) * head_dim)

    def local_part():
        for h in range(heads):
            lo, hi = h * head_dim, (h + 1) * head_dim
            _, _, decays, top = gate_parts(h)
            scores = dot(qs[:, lo:hi], ks[:, lo:hi], ((1,), (1,))) * scale * jnp.exp(decays - top)
            den[h] = jnp.broadcast_to(jnp.sum(scores, axis=1, keepdims=True), (count, GROUP))
            num[h] = dot(scores.astype(BF16), vs[:, lo:hi])

        @pl.when(sp > 0)
        def _():
            edge.wait_recv()

        @pl.when(sp == 0)
        def _():
            halo[...] = jnp.zeros(halo.shape, BF16)
        pad[0:EXTRA, :] = halo[...].astype(F32)
        pad[EXTRA:EXTRA + count, :] = mixed[...].astype(F32)
        reach = taps.shape[0] - 1
        tap = taps[...].astype(F32)
        acc = tap[0:1, :] * pad[EXTRA - reach:EXTRA - reach + count, :]
        for j in range(1, reach + 1):
            acc = acc + tap[j:j + 1, :] * pad[EXTRA - reach + j:EXTRA - reach + j + count, :]
        yc[...] = (gb[...].astype(F32) * acc).astype(BF16)

    early = pair >= (last_pair + 1) // 2
    pl.when(early)(local_part)

    is_odd = odd == 1

    @pl.when(pair == 0)
    def _():
        for h in range(heads):
            got_p[h] = jnp.zeros((head_dim, head_dim), BF16)
            meta_p[h] = jnp.full((8, head_dim), 0.0, F32)
            meta_p[h, 1:2, :] = jnp.full((1, head_dim), LOWEST, F32)

    def chain(h, c):
        at = pl.ds(c * rows, rows)
        if c == NCHUNK:
            return remote(meta_s.at[h], meta_p.at[h], p_s.at[h, c], p_r.at[h, c], (sp + 2, tp))
        return remote(put_p.at[h, at], got_p.at[h, at], p_s.at[h, c], p_r.at[h, c], (sp + 2, tp))

    def pair_copy(h, c):
        return a_sends[h * (NCHUNK + 1) + (0 if c == NCHUNK else c + 1)]

    for h in range(heads):
        pair_copy(h, NCHUNK).wait_recv()
        pl.when(pair > 0)(chain(h, NCHUNK).wait_recv)
        own, got, before = meta[h], meta_a[h], meta_p[h]
        first = jnp.where(is_odd, got, own)
        second = jnp.where(is_odd, own, got)
        m_p, m_e, m_o = before[1:2, :], first[1:2, :], second[1:2, :]
        b_e, b_o = first[2:3, :], second[2:3, :]
        m_1 = jnp.maximum(b_e + m_p, m_e)
        m_2 = jnp.maximum(b_o + m_1, m_o)
        c_p = jnp.exp(b_o + (b_e + m_p) - m_2)
        c_e = jnp.exp(b_o + m_e - m_2)
        c_o = jnp.exp(m_o - m_2)
        meta_s[h] = jnp.zeros((8, head_dim), F32)
        meta_s[h, 0:1, :] = c_p * before[0:1, :] + c_e * first[0:1, :] + c_o * second[0:1, :]
        meta_s[h, 1:2, :] = m_2
        pl.when(pair < last_pair)(chain(h, NCHUNK).start)
        c_own = jnp.where(is_odd, c_o, c_e)
        c_got = jnp.where(is_odd, c_e, c_o)
        f_p = jnp.where(is_odd, jnp.exp(b_e + m_p - m_1), 1.0)
        f_e = jnp.where(is_odd, jnp.exp(m_e - m_1), 0.0)
        meta_in = (f_p * before[0:1, :] + f_e * first[0:1, :], jnp.where(is_odd, m_1, m_p))
        meta_i[h, 0:1, :] = meta_in[0]
        meta_i[h, 1:2, :] = meta_in[1]
        for c in range(NCHUNK):
            at = pl.ds(c * rows, rows)
            pair_copy(h, c).wait_recv()
            pl.when(pair > 0)(chain(h, c).wait_recv)
            block_p = got_p[h, at, :].astype(F32)
            block_a = got_a[h, at, :].astype(F32)
            put_p[h, at, :] = (c_p * block_p + c_own * own_c[h, at, :].astype(F32) + c_got * block_a).astype(BF16)
            pl.when(pair < last_pair)(chain(h, c).start)
            in_c[h, at, :] = (f_p * block_p + f_e * block_a).astype(BF16)

    pl.when(jnp.logical_not(early))(local_part)

    own_sq = jnp.zeros((count, 1), F32)
    for h in range(heads):
        lo, hi = h * head_dim, (h + 1) * head_dim
        _, b_col, _, top_own = gate_parts(h)
        n_in, m_in = meta_i[h, 0:1, :], meta_i[h, 1:2, 0:1]
        top = jnp.maximum(top_own, b_col + m_in)
        s_own = jnp.exp(top_own - top)
        s_in = jnp.exp(b_col + m_in - top)
        qh = qs[:, lo:hi]
        den_all = s_own * den[h, :, 0:1] + s_in * jnp.sum(qh.astype(F32) * n_in, axis=1, keepdims=True)
        num_all = s_own * num[h] + s_in * dot(qh, in_c[h])
        raw = num_all / jnp.maximum(jnp.abs(den_all), jnp.exp(-top))
        num[h] = raw
        own_sq = own_sq + jnp.sum(raw * raw, axis=1, keepdims=True)
    sq_own[...] = jnp.broadcast_to(own_sq, (count, GROUP)).T[0:8, :]
    sq_sends = []
    for k, other in enumerate(others):
        copy = remote(sq_own, sq_got.at[tp], q_s.at[k], q_r.at[tp], (sp, other))
        copy.start()
        sq_sends.append(copy)
    total_sq = sq_own[...]
    for k, other in enumerate(others):
        remote(sq_own, sq_got.at[other], q_s.at[k], q_r.at[other], (sp, other)).wait_recv()
        total_sq = total_sq + sq_got[other]
    features = n_tp * heads * head_dim
    norm_row = lax.rsqrt(total_sq[0:1, :] / features + EPS)
    norm = jnp.broadcast_to(norm_row, (count, count)).T[:, 0:1]
    for h in range(heads):
        lo, hi = h * head_dim, (h + 1) * head_dim
        normed = num[h] * norm * mgain[:, lo:hi].astype(F32)
        sig = 1.0 / (1.0 + jnp.exp(-og[:, lo:hi].astype(F32)))
        ym[:, lo:hi] = (sig * normed).astype(BF16)

    wait_of["co"].wait()
    wait_of["mo"].wait()
    share = count // n_tp
    width = model // NOUT
    out_sends = []
    for j in range(NOUT):
        at = pl.ds(j * width, width)
        part[:, j * width:(j + 1) * width] = (
            dot(yc[...], vco[:, j * width:(j + 1) * width]) + dot(ym[...], vmo[:, j * width:(j + 1) * width])
        ).astype(BF16)
        for k, other in enumerate(others):
            mine = pl.ds(pl.multiple_of(other * share, share), share)
            copy = remote(part.at[mine, at], rs.at[tp, :, at], r_s.at[j, k], r_r.at[j, tp], (sp, other))
            copy.start()
            out_sends.append(copy)
    mine = pl.ds(pl.multiple_of(tp * share, share), share)
    for j in range(NOUT):
        at = pl.ds(j * width, width)
        acc = part[mine, j * width:(j + 1) * width].astype(F32)
        for k, other in enumerate(others):
            remote(part.at[mine, at], rs.at[other, :, at], r_s.at[j, k], r_r.at[j, other], (sp, other)).wait_recv()
            acc = acc + rs[other, :, j * width:(j + 1) * width].astype(F32)
        out[:, j * width:(j + 1) * width] = acc.astype(BF16)

    for copy in tok_sends + a_sends + sq_sends + out_sends:
        copy.wait_send()
    pl.when(sp < n_sp - 1)(edge.wait_send)

    @pl.when(pair < last_pair)
    def _():
        for h in range(heads):
            for c in range(NCHUNK + 1):
                chain(h, c).wait_send()


def body(n_sp, n_tp, tokens, norm_gain, conv_b_w, conv_c_w, conv_u_w, conv_taps, query_w, key_w,
         value_w, outgate_w, gate_w, gate_bias, mem_gain, conv_out_w, mem_out_w):
    count, feats = tokens.shape
    model, conv = conv_b_w.shape
    mem = query_w.shape[1]
    heads = gate_bias.shape[1]
    head_dim = mem // heads
    share = count // n_tp
    gates_w = jnp.transpose(gate_w, (1, 2, 0)).reshape(2 * heads, model)
    gates_w = jnp.pad(gates_w, ((0, GROUP - 2 * heads), (0, 0)))
    bias = jnp.pad(gate_bias.reshape(1, 2 * heads), ((0, 0), (0, GROUP - 2 * heads)))
    vmem, hbm = pl.BlockSpec(memory_space=pltpu.VMEM), pl.BlockSpec(memory_space=pl.ANY)
    V, S = pltpu.VMEM, pltpu.SemaphoreType.DMA
    state = V((heads, head_dim, head_dim), BF16)
    small = V((heads, 8, head_dim), F32)
    scratch = [
        V((n_tp, count + EXTRA, feats), BF16), V((count, model), BF16),
        V((model, conv), BF16), V((model, conv), BF16), V((model, conv), BF16),
        V((model, mem), BF16), V((model, mem), BF16), V((model, mem), BF16), V((model, mem), BF16),
        V((GROUP, model), BF16), V((conv, model), BF16), V((mem, model), BF16),
        V((count, mem), BF16), V((count, mem), BF16), V((count, mem), BF16), V((count, mem), BF16),
        state, state, state, state, state,
        small, small, small, small, small, V((count, GROUP), F32), V((GROUP, count), F32),
        V((heads, count, head_dim), F32), V((heads, count, GROUP), F32),
        V((count, conv), BF16), V((count, conv), BF16), V((EXTRA, conv), BF16), V((count + EXTRA, conv), F32),
        V((count, conv), BF16), V((count, mem), BF16),
        V((8, count), F32), V((n_tp, 8, count), F32),
        V((count, model), BF16), V((n_tp, share, model), BF16),
        S((10,)), S, S((n_tp,)), S((n_tp,)),
        S((heads, NCHUNK + 1)), S((heads, NCHUNK + 1)), S((heads, NCHUNK + 1)), S((heads, NCHUNK + 1)),
        S, S, S((n_tp,)), S((n_tp,)), S((NOUT, n_tp)), S((NOUT, n_tp)),
    ]
    return pl.pallas_call(
        functools.partial(kernel, n_sp, n_tp, heads),
        out_shape=jax.ShapeDtypeStruct((share, model), BF16),
        in_specs=[hbm, vmem, hbm, hbm, hbm, vmem, hbm, hbm, hbm, hbm, hbm, vmem, vmem, hbm, hbm],
        out_specs=vmem,
        scratch_shapes=scratch,
        compiler_params=pltpu.CompilerParams(
            collective_id=0, has_side_effects=True, vmem_limit_bytes=60 * 1024 * 1024),
        name="mixer",
    )(tokens, norm_gain, conv_b_w, conv_c_w, conv_u_w, conv_taps, query_w, key_w, value_w, outgate_w,
      gates_w, bias, mem_gain.reshape(1, mem), conv_out_w, mem_out_w)


def solution(mesh):
    n_sp, n_tp = mesh.shape["sp"], mesh.shape["tp"]
    cols, rows = P(None, "tp"), P("tp", None)
    return jax.shard_map(
        functools.partial(body, n_sp, n_tp),
        mesh=mesh,
        in_specs=(
            P("sp", "tp"), cols, cols, cols, cols, cols, cols, cols, cols, cols,
            P(None, None, "tp"), cols, P("tp"), rows, rows,
        ),
        out_specs=P(("sp", "tp"), None),
        check_vma=False,
    )
```

time: 150 us -> 48.2 us (0.32); the launches traced: 147 us -> 47.9 us
  blocking collectives: 55.1 us -> 0 us
  waiting for transfers between devices: 43.4 us -> 0 us
  Pallas kernels: 0 us -> 42.2 us
  matrix products: 17.4 us -> 0 us
  between operations: 14.3 us -> 0.01 us
  other arithmetic: 10.4 us -> 0 us
  starting transfers between devices: 3.19 us -> 0 us
  local copies, waits for them, and re-layouts: 2.92 us -> 5.68 us
    pallas_call x0 -> x1, Pallas kernels: none -> 42.2 us  [body(): pl.pallas_call(functools.partial(kernel, n_sp, n_tp, heads), out_shape=ja...]
    all_gather x3 -> x0, blocking collectives: 32.6 us -> none  [the longest x1 19.2 us: prefix(): pieces = jax.tree.map(lambda part: lax.all_gather(part, axis), value)]
    reduce_scatter x1 -> x0, waiting for transfers between devices: 21.9 us -> none  [body(): lax.psum_scatter((jnp.dot(y_conv, conv_out_w, preferred_element_type=jnp....]
    all_gather x1 -> x0, waiting for transfers between devices: 21.4 us -> none  [prefix(): pieces = jax.tree.map(lambda part: lax.all_gather(part, axis), value)]
    dot_general x18 -> x0, matrix products: 17.4 us -> none  [the longest x8 9.01 us: body(): jnp.dot(scaled, weight, preferred_element_type=jnp.float32)]
    unnamed x1 -> x0, blocking collectives: 16.8 us -> none
    select_n x14 -> x0, other arithmetic: 8.88 us -> none  [prefix_step(): jnp.where(position < mine, new, old)]
    psum x1 -> x0, blocking collectives: 5.74 us -> none  [body(): all_squares = lax.psum(own_squares, 'tp')]
  transfers between devices with their start and end apart: 3 -> 0, of which waited for: 2 -> 0; matrix products, arithmetic and copies ran while one was open for 8% -> 0% of each run, Pallas kernels for 0% -> 0%
where the time goes in v1:
time: 48.2 us; the launch traced here: 47.9 us
  Pallas kernels  42.2 us (88%)
  local copies, waits for them, and re-layouts  5.68 us (12%)
    pallas_call x1, Pallas kernels, body(): pl.pallas_call(functools.partial(kernel, n_sp, n_tp, heads), out_shape=ja...  42.2 us
    unnamed x1, local copies, waits for them, and re-layouts  1.57 us
    reshape x1, local copies, waits for them, and re-layouts, body(): mem_gain.reshape(1, mem)  1.26 us

profile of v1, /device:TPU:25, one launch (start us, length us, event | category | flops | bytes accessed | tf_op | source)
XLA Modules:
  0.0 47.9 jit_solution(5457944952020237176)
XLA Ops:
  0.0 0.8 %reshape.10 = f32[1,4]{1,0:T(1,128)S(1)} reshape(f32[2,2]{1,0:T(2,128)} %param.26) | data formatting | bytes 32 | tf_op jit(solution)/shard_map/reshape | solution.py:335
  0.8 0.5 %pad.9.refs_11_ = f32[1,128]{1,0:T(1,128)} pad(f32[1,4]{1,0:T(1,128)S(1)} %reshape.10, f32[]{:T(128)} %constant.4.clone.1), padding=0_0x0_124 | pad | bytes 532 | tf_op jit(solution)/shard_map/jit(_pad)/pad | solution.py:335
  1.3 1.3 %reshape.11.refs_12_ = bf16[1,512]{1,0:T(2,128)(2,1)} reshape(bf16[512]{0:T(512)(128)(2,1)} %param.27) | data formatting | bytes 2048 | tf_op jit(solution)/shard_map/reshape | solution.py:367
  2.5 0.7 %reshape.9 = bf16[4,2048]{1,0:T(4,128)(2,1)S(1)} reshape(bf16[2,2,2048]{2,1,0:T(2,128)(2,1)} %bitcast.1) | data formatting | bytes 32768 | tf_op jit(solution)/shard_map/reshape | solution.py:333
  3.3 0.8 %pad.8.refs_10_ = bf16[128,2048]{1,0:T(8,128)(2,1)} pad(bf16[4,2048]{1,0:T(4,128)(2,1)S(1)} %reshape.9, bf16[]{:T(256)} %constant.3.clone.1), padding=0_124x0_0 | pad | bytes 540674 | tf_op jit(solution)/shard_map/jit(_pad)/pad | solution.py:334
  4.1 42.2 %mixer.1 = bf16[32,2048]{1,0:T(8,128)(2,1)} custom-call(bf16[128,512]{1,0:T(8,128)(2,1)} %refs_0_.1, bf16[1,512]{1,0:T(2,128)(2,1)} %refs_1_.1, bf16[2048,256]{1,0:T(8,128)(2,1)} %refs_2_.1, bf16[2048,256]{1,0:T(8,128)(2,1)} %refs_3_.1, bf16[2048,256]{1,0:T(8,128)(2,1)} %refs_4_.1, bf16[3,256]{1,0:T(4,128)(2,1)} %refs_5_.1, bf16[2048,512]{1,0:T(8,128)(2,1)} %refs_6_.1, ...), custom_call_target="tpu_custom_call" | custom-call | tf_op jit(solution)/shard_map/mixer/pallas_call | solution.py:357
  46.3 1.6 %copy.17 = bf16[32,2048]{1,0:T(8,128)(2,1)} copy(bf16[32,2048]{1,0:T(8,128)(2,1)} %mixer.1) | data formatting | bytes 262144

commit v2 on v1

--- a/solution.py
+++ b/solution.py
@@ -26,7 +26,7 @@
 def kernel(n_sp, n_tp, heads, *refs):
     (tok, gain, wb, wc, wu, taps, wq, wk, wv, wo, gw, bias, mgain, cow, mow, out) = refs[:16]
     (
-        full, scaled, vb, vc, vu, vq, vk, vv, vo, vg, vco, vmo,
+        full, scaled, vb, vc, vu, vq, vk, vv, vo, vg, raw_g, raw_b, vco, vmo,
         qs, ks, vs, og, own_c, got_a, got_p, put_p, in_c,
         meta, meta_a, meta_p, meta_s, meta_i, gates, gates_t,
         num, den, gb, mixed, halo, pad, yc, ym, sq_own, sq_got, part, rs,
@@ -50,13 +50,21 @@
     loads = [
         pltpu.make_async_copy(src, dst, sem_w.at[i])
         for i, (src, dst) in enumerate(
-            ((gw, vg), (wk, vk), (wv, vv), (wq, vq), (wc, vc), (wu, vu), (wb, vb), (wo, vo), (cow, vco), (mow, vmo))
+            ((wk, vk), (wv, vv), (wq, vq), (wc, vc), (wu, vu), (wb, vb), (wo, vo), (cow, vco), (mow, vmo))
         )
     ]
     for load in loads:
         load.start()
-    wait_of = dict(zip(("g", "k", "v", "q", "c", "u", "b", "o", "co", "mo"), loads))
+    wait_of = dict(zip(("k", "v", "q", "c", "u", "b", "o", "co", "mo"), loads))
     full[tp, pl.ds(count, EXTRA), :] = jnp.broadcast_to(gain[...].astype(F32), (EXTRA, feats)).astype(BF16)
+
+    raw_g[...] = jnp.zeros(raw_g.shape, F32)
+    raw_b[...] = jnp.zeros(raw_b.shape, F32)
+    for i in range(2):
+        raw_g[i * heads:(i + 1) * heads, :] = gw[i].astype(F32)
+        raw_b[0:1, i * heads:(i + 1) * heads] = bias[i:i + 1, :]
+    vg[0:EXTRA, :] = raw_g[...].astype(BF16)
+    vg[EXTRA:GROUP, :] = jnp.zeros((GROUP - EXTRA, model), BF16)
 
     barrier = pltpu.get_barrier_semaphore()
     steps = (1, -1, 2, -2)
@@ -106,8 +114,7 @@
     def project(ref, lo, hi):
         return (inv * dot(scaled[...], ref[:, lo:hi])).astype(BF16)
 
-    wait_of["g"].wait()
-    pre = inv * dot(scaled[...], vg[...], ((1,), (1,))) + bias[0:1, :]
+    pre = inv * dot(scaled[...], vg[...], ((1,), (1,))) + raw_b[0:1, :]
     lf = jnp.minimum(pre, 0.0) - jnp.log1p(jnp.exp(-jnp.abs(pre)))
     row_id = lax.broadcasted_iota(jnp.int32, (count, count), 0)
     col_id = lax.broadcasted_iota(jnp.int32, (count, count), 1)
@@ -283,7 +290,7 @@
     norm = jnp.broadcast_to(norm_row, (count, count)).T[:, 0:1]
     for h in range(heads):
         lo, hi = h * head_dim, (h + 1) * head_dim
-        normed = num[h] * norm * mgain[:, lo:hi].astype(F32)
+        normed = num[h] * norm * mgain[lo:hi].astype(F32).reshape(1, head_dim)
         sig = 1.0 / (1.0 + jnp.exp(-og[:, lo:hi].astype(F32)))
         ym[:, lo:hi] = (sig * normed).astype(BF16)
 
@@ -330,9 +337,7 @@
     heads = gate_bias.shape[1]
     head_dim = mem // heads
     share = count // n_tp
-    gates_w = jnp.transpose(gate_w, (1, 2, 0)).reshape(2 * heads, model)
-    gates_w = jnp.pad(gates_w, ((0, GROUP - 2 * heads), (0, 0)))
-    bias = jnp.pad(gate_bias.reshape(1, 2 * heads), ((0, 0), (0, GROUP - 2 * heads)))
+    gates_w = jnp.transpose(gate_w, (1, 2, 0))
     vmem, hbm = pl.BlockSpec(memory_space=pltpu.VMEM), pl.BlockSpec(memory_space=pl.ANY)
     V, S = pltpu.VMEM, pltpu.SemaphoreType.DMA
     state = V((heads, head_dim, head_dim), BF16)
@@ -341,7 +346,7 @@
         V((n_tp, count + EXTRA, feats), BF16), V((count, model), BF16),
         V((model, conv), BF16), V((model, conv), BF16), V((model, conv), BF16),
         V((model, mem), BF16), V((model, mem), BF16), V((model, mem), BF16), V((model, mem), BF16),
-        V((GROUP, model), BF16), V((conv, model), BF16), V((mem, model), BF16),
+        V((GROUP, model), BF16), V((EXTRA, model), F32), V((8, GROUP), F32), V((conv, model), BF16), V((mem, model), BF16),
         V((count, mem), BF16), V((count, mem), BF16), V((count, mem), BF16), V((count, mem), BF16),
         state, state, state, state, state,
         small, small, small, small, small, V((count, GROUP), F32), V((GROUP, count), F32),
@@ -350,21 +355,21 @@
         V((count, conv), BF16), V((count, mem), BF16),
         V((8, count), F32), V((n_tp, 8, count), F32),
         V((count, model), BF16), V((n_tp, share, model), BF16),
-        S((10,)), S, S((n_tp,)), S((n_tp,)),
+        S((9,)), S, S((n_tp,)), S((n_tp,)),
         S((heads, NCHUNK + 1)), S((heads, NCHUNK + 1)), S((heads, NCHUNK + 1)), S((heads, NCHUNK + 1)),
         S, S, S((n_tp,)), S((n_tp,)), S((NOUT, n_tp)), S((NOUT, n_tp)),
     ]
     return pl.pallas_call(
         functools.partial(kernel, n_sp, n_tp, heads),
         out_shape=jax.ShapeDtypeStruct((share, model), BF16),
-        in_specs=[hbm, vmem, hbm, hbm, hbm, vmem, hbm, hbm, hbm, hbm, hbm, vmem, vmem, hbm, hbm],
+        in_specs=[hbm, vmem, hbm, hbm, hbm, vmem, hbm, hbm, hbm, hbm, vmem, vmem, vmem, hbm, hbm],
         out_specs=vmem,
         scratch_shapes=scratch,
         compiler_params=pltpu.CompilerParams(
             collective_id=0, has_side_effects=True, vmem_limit_bytes=60 * 1024 * 1024),
         name="mixer",
     )(tokens, norm_gain, conv_b_w, conv_c_w, conv_u_w, conv_taps, query_w, key_w, value_w, outgate_w,
-      gates_w, bias, mem_gain.reshape(1, mem), conv_out_w, mem_out_w)
+      gates_w, gate_bias, mem_gain, conv_out_w, mem_out_w)
 
 
 def solution(mesh):

time: 48.2 us -> 43 us (0.89)
  local copies, waits for them, and re-layouts: 5.68 us -> 1.57 us
  Pallas kernels: 42.2 us -> 41.3 us
    reshape x3 -> x0, local copies, waits for them, and re-layouts: 2.75 us -> none  [the longest x1 1.26 us: body(): mem_gain.reshape(1, mem)]
    pad x2 -> x0, local copies, waits for them, and re-layouts: 1.37 us -> none  [the longest x1 0.84 us: body(): gates_w = jnp.pad(gates_w, ((0, GROUP - 2 * heads), (0, 0)))]
    pallas_call x1, Pallas kernels: 42.2 us -> 41.3 us  [body(): pl.pallas_call(functools.partial(kernel, n_sp, n_tp, heads), out_shape=ja...]
where the time goes in v2:
time: 43 us; the launch traced here: 42.8 us
  Pallas kernels  41.3 us (96%)
  local copies, waits for them, and re-layouts  1.57 us (4%)
    pallas_call x1, Pallas kernels, body(): pl.pallas_call(functools.partial(kernel, n_sp, n_tp, heads), out_shape=ja...  41.3 us
    unnamed x1, local copies, waits for them, and re-layouts  1.57 us

profile of v2, /device:TPU:25, one launch (start us, length us, event | category | flops | bytes accessed | tf_op | source)
XLA Modules:
  0.0 42.8 jit_solution(3218568593435156750)
XLA Ops:
  0.0 41.3 %mixer.1 = bf16[32,2048]{1,0:T(8,128)(2,1)} custom-call(bf16[128,512]{1,0:T(8,128)(2,1)} %refs_0_.1, bf16[1,512]{1,0:T(2,128)(2,1)} %refs_1_.1, bf16[2048,256]{1,0:T(8,128)(2,1)} %refs_2_.1, bf16[2048,256]{1,0:T(8,128)(2,1)} %refs_3_.1, bf16[2048,256]{1,0:T(8,128)(2,1)} %refs_4_.1, bf16[3,256]{1,0:T(4,128)(2,1)} %refs_5_.1, bf16[2048,512]{1,0:T(8,128)(2,1)} %refs_6_.1, ...), custom_call_target="tpu_custom_call" | custom-call | tf_op jit(solution)/shard_map/mixer/pallas_call | solution.py:362
  41.3 1.6 %copy.17 = bf16[32,2048]{1,0:T(8,128)(2,1)} copy(bf16[32,2048]{1,0:T(8,128)(2,1)} %mixer.1) | data formatting | bytes 262144

commit v3 on v2

--- a/solution.py
+++ b/solution.py
@@ -29,8 +29,8 @@
         full, scaled, vb, vc, vu, vq, vk, vv, vo, vg, raw_g, raw_b, vco, vmo,
         qs, ks, vs, og, own_c, got_a, got_p, put_p, in_c,
         meta, meta_a, meta_p, meta_s, meta_i, gates, gates_t,
-        num, den, gb, mixed, halo, pad, yc, ym, sq_own, sq_got, part, rs,
-        sem_w, sem_tok, tok_s, tok_r, a_s, a_r, p_s, p_r, h_s, h_r, q_s, q_r, r_s, r_r,
+        num, den, gb, mixed, halo, pad, yc, ym, sq_own, sq_got, part, rs, acc_c, acc_m, from_mate, summed,
+        sem_w, sem_tok, tok_s, tok_r, a_s, a_r, p_s, p_r, h_s, h_r, q_s, q_r, r_s, r_r, d_s, d_r,
     ) = refs[16:]
     sp, tp = lax.axis_index("sp"), lax.axis_index("tp")
     count, feats = tok.shape
@@ -97,18 +97,22 @@
     for k, x in enumerate(far):
         tok_sends.append(send_tok(tp, x * 2 + core, k))
     tok_sends.append(send_tok(tp, mate, chips - 1))
+    def take(source):
+        wide = full[source, 0:count, :].astype(F32)
+        gains = full[source, count:count + 1, :].astype(F32)
+        scaled[:, pl.ds(pl.multiple_of(source * feats, GROUP), feats)] = (wide * gains).astype(BF16)
+        return jnp.sum(wide * wide, axis=1, keepdims=True)
+
+    squares = take(tp)
+    got_tok(mate)
+    squares = squares + take(mate)
     for k, x in enumerate(far):
         got_tok(x * 2 + core)
         tok_sends.append(send_tok(x * 2 + core, mate, chips + k))
-    got_tok(mate)
+        squares = squares + take(x * 2 + core)
     for k, x in enumerate(far):
         got_tok(x * 2 + 1 - core)
-
-    squares = jnp.zeros((count, 1), F32)
-    for s in range(n_tp):
-        wide = full[s, 0:count, :].astype(F32)
-        scaled[:, s * feats:(s + 1) * feats] = (wide * full[s, count:count + 1, :].astype(F32)).astype(BF16)
-        squares = squares + jnp.sum(wide * wide, axis=1, keepdims=True)
+        squares = squares + take(x * 2 + 1 - core)
     inv = lax.rsqrt(squares / model + EPS)
 
     def project(ref, lo, hi):
@@ -273,14 +277,23 @@
         den_all = s_own * den[h, :, 0:1] + s_in * jnp.sum(qh.astype(F32) * n_in, axis=1, keepdims=True)
         num_all = s_own * num[h] + s_in * dot(qh, in_c[h])
         raw = num_all / jnp.maximum(jnp.abs(den_all), jnp.exp(-top))
-        num[h] = raw
         own_sq = own_sq + jnp.sum(raw * raw, axis=1, keepdims=True)
+        sig = 1.0 / (1.0 + jnp.exp(-og[:, lo:hi].astype(F32)))
+        ym[:, lo:hi] = (sig * raw * mgain[lo:hi].astype(F32).reshape(1, head_dim)).astype(BF16)
     sq_own[...] = jnp.broadcast_to(own_sq, (count, GROUP)).T[0:8, :]
     sq_sends = []
     for k, other in enumerate(others):
         copy = remote(sq_own, sq_got.at[tp], q_s.at[k], q_r.at[tp], (sp, other))
         copy.start()
         sq_sends.append(copy)
+    wait_of["co"].wait()
+    wait_of["mo"].wait()
+    share = count // n_tp
+    width = model // NOUT
+    for j in range(NOUT):
+        lo, hi = j * width, (j + 1) * width
+        acc_c[:, lo:hi] = dot(yc[...], vco[:, lo:hi])
+        acc_m[:, lo:hi] = dot(ym[...], vmo[:, lo:hi])
     total_sq = sq_own[...]
     for k, other in enumerate(others):
         remote(sq_own, sq_got.at[other], q_s.at[k], q_r.at[other], (sp, other)).wait_recv()
@@ -288,35 +301,45 @@
     features = n_tp * heads * head_dim
     norm_row = lax.rsqrt(total_sq[0:1, :] / features + EPS)
     norm = jnp.broadcast_to(norm_row, (count, count)).T[:, 0:1]
-    for h in range(heads):
-        lo, hi = h * head_dim, (h + 1) * head_dim
-        normed = num[h] * norm * mgain[lo:hi].astype(F32).reshape(1, head_dim)
-        sig = 1.0 / (1.0 + jnp.exp(-og[:, lo:hi].astype(F32)))
-        ym[:, lo:hi] = (sig * normed).astype(BF16)
-
-    wait_of["co"].wait()
-    wait_of["mo"].wait()
-    share = count // n_tp
-    width = model // NOUT
+    def block(x, y):
+        return pl.ds(pl.multiple_of((x * 2 + y) * share, share), share)
+
+    def mate_copy(j, x):
+        at = pl.ds(j * width, width)
+        return remote(part.at[block(x, 1 - core), at], from_mate.at[x, :, at], d_s.at[j, x], d_r.at[j, x], (sp, mate))
+
+    def far_copy(j, x):
+        at = pl.ds(j * width, width)
+        return remote(summed.at[x, :, at], rs.at[chip, :, at], r_s.at[j, x], r_r.at[j, chip], (sp, x * 2 + core))
+
     out_sends = []
     for j in range(NOUT):
-        at = pl.ds(j * width, width)
-        part[:, j * width:(j + 1) * width] = (
-            dot(yc[...], vco[:, j * width:(j + 1) * width]) + dot(ym[...], vmo[:, j * width:(j + 1) * width])
-        ).astype(BF16)
-        for k, other in enumerate(others):
-            mine = pl.ds(pl.multiple_of(other * share, share), share)
-            copy = remote(part.at[mine, at], rs.at[tp, :, at], r_s.at[j, k], r_r.at[j, tp], (sp, other))
+        lo, hi = j * width, (j + 1) * width
+        part[:, lo:hi] = (acc_c[:, lo:hi] + norm * acc_m[:, lo:hi]).astype(BF16)
+        for x in far + [chip]:
+            copy = mate_copy(j, x)
             copy.start()
             out_sends.append(copy)
-    mine = pl.ds(pl.multiple_of(tp * share, share), share)
+
+    def both_cores(j, x):
+        lo, hi = j * width, (j + 1) * width
+        mate_copy(j, x).wait_recv()
+        return part[block(x, core), lo:hi].astype(F32) + from_mate[x, :, lo:hi].astype(F32)
+
     for j in range(NOUT):
-        at = pl.ds(j * width, width)
-        acc = part[mine, j * width:(j + 1) * width].astype(F32)
-        for k, other in enumerate(others):
-            remote(part.at[mine, at], rs.at[other, :, at], r_s.at[j, k], r_r.at[j, other], (sp, other)).wait_recv()
-            acc = acc + rs[other, :, j * width:(j + 1) * width].astype(F32)
-        out[:, j * width:(j + 1) * width] = acc.astype(BF16)
+        for x in far:
+            summed[x, :, j * width:(j + 1) * width] = both_cores(j, x).astype(BF16)
+            copy = far_copy(j, x)
+            copy.start()
+            out_sends.append(copy)
+    for j in range(NOUT):
+        lo, hi = j * width, (j + 1) * width
+        at = pl.ds(lo, width)
+        acc = both_cores(j, chip)
+        for x in far:
+            remote(summed.at[x, :, at], rs.at[x, :, at], r_s.at[j, x], r_r.at[j, x], (sp, x * 2 + core)).wait_recv()
+            acc = acc + rs[x, :, lo:hi].astype(F32)
+        out[:, lo:hi] = acc.astype(BF16)
 
     for copy in tok_sends + a_sends + sq_sends + out_sends:
         copy.wait_send()
@@ -336,7 +359,7 @@
     mem = query_w.shape[1]
     heads = gate_bias.shape[1]
     head_dim = mem // heads
-    share = count // n_tp
+    share, chips = count // n_tp, n_tp // 2
     gates_w = jnp.transpose(gate_w, (1, 2, 0))
     vmem, hbm = pl.BlockSpec(memory_space=pltpu.VMEM), pl.BlockSpec(memory_space=pl.ANY)
     V, S = pltpu.VMEM, pltpu.SemaphoreType.DMA
@@ -354,10 +377,11 @@
         V((count, conv), BF16), V((count, conv), BF16), V((EXTRA, conv), BF16), V((count + EXTRA, conv), F32),
         V((count, conv), BF16), V((count, mem), BF16),
         V((8, count), F32), V((n_tp, 8, count), F32),
-        V((count, model), BF16), V((n_tp, share, model), BF16),
+        V((count, model), BF16), V((chips, share, model), BF16),
+        V((count, model), F32), V((count, model), F32), V((chips, share, model), BF16), V((chips, share, model), BF16),
         S((9,)), S, S((n_tp,)), S((n_tp,)),
         S((heads, NCHUNK + 1)), S((heads, NCHUNK + 1)), S((heads, NCHUNK + 1)), S((heads, NCHUNK + 1)),
-        S, S, S((n_tp,)), S((n_tp,)), S((NOUT, n_tp)), S((NOUT, n_tp)),
+        S, S, S((n_tp,)), S((n_tp,)), S((NOUT, chips)), S((NOUT, chips)), S((NOUT, chips)), S((NOUT, chips)),
     ]
     return pl.pallas_call(
         functools.partial(kernel, n_sp, n_tp, heads),

time: 43 us -> 41.1 us (0.956)
  Pallas kernels: 41.3 us -> 39.3 us
    pallas_call x1, Pallas kernels: 41.3 us -> 39.3 us  [body(): pl.pallas_call(functools.partial(kernel, n_sp, n_tp, heads), out_shape=ja...]
where the time goes in v3:
time: 41.1 us; the launch traced here: 40.9 us
  Pallas kernels  39.3 us (96%)
  local copies, waits for them, and re-layouts  1.57 us (4%)
    pallas_call x1, Pallas kernels, body(): pl.pallas_call(functools.partial(kernel, n_sp, n_tp, heads), out_shape=ja...  39.3 us
    unnamed x1, local copies, waits for them, and re-layouts  1.57 us

profile of v3, /device:TPU:25, one launch (start us, length us, event | category | flops | bytes accessed | tf_op | source)
XLA Modules:
  0.0 40.9 jit_solution(3370999056836461662)
XLA Ops:
  0.0 39.3 %mixer.1 = bf16[32,2048]{1,0:T(8,128)(2,1)} custom-call(bf16[128,512]{1,0:T(8,128)(2,1)} %refs_0_.1, bf16[1,512]{1,0:T(2,128)(2,1)} %refs_1_.1, bf16[2048,256]{1,0:T(8,128)(2,1)} %refs_2_.1, bf16[2048,256]{1,0:T(8,128)(2,1)} %refs_3_.1, bf16[2048,256]{1,0:T(8,128)(2,1)} %refs_4_.1, bf16[3,256]{1,0:T(4,128)(2,1)} %refs_5_.1, bf16[2048,512]{1,0:T(8,128)(2,1)} %refs_6_.1, ...), custom_call_target="tpu_custom_call" | custom-call | tf_op jit(solution)/shard_map/mixer/pallas_call | solution.py:386
  39.3 1.6 %copy.17 = bf16[32,2048]{1,0:T(8,128)(2,1)} copy(bf16[32,2048]{1,0:T(8,128)(2,1)} %mixer.1) | data formatting | bytes 262144

commit v4 on v3

--- a/solution.py
+++ b/solution.py
@@ -14,8 +14,8 @@
 F32 = jnp.float32
 BF16 = jnp.bfloat16
 GROUP = 128
-NCHUNK = 4
-NOUT = 4
+NCHUNK = 8
+NOUT = 2
 EXTRA = 16
 
 
@@ -97,13 +97,25 @@
     for k, x in enumerate(far):
         tok_sends.append(send_tok(tp, x * 2 + core, k))
     tok_sends.append(send_tok(tp, mate, chips - 1))
-    def take(source):
+    mem = wk.shape[1]
+    wait_of["k"].wait()
+    wait_of["v"].wait()
+
+    def take(source, first=False):
         wide = full[source, 0:count, :].astype(F32)
         gains = full[source, count:count + 1, :].astype(F32)
-        scaled[:, pl.ds(pl.multiple_of(source * feats, GROUP), feats)] = (wide * gains).astype(BF16)
+        piece = (wide * gains).astype(BF16)
+        at = pl.ds(pl.multiple_of(source * feats, GROUP), feats)
+        scaled[:, at] = piece
+        for lo, hi, update in (
+            (2 * mem, 2 * mem + GROUP, dot(piece, vg[:, at], ((1,), (1,)))),
+            (0, mem, dot(piece, vk[at, :])),
+            (mem, 2 * mem, dot(piece, vv[at, :])),
+        ):
+            acc_c[:, lo:hi] = update if first else acc_c[:, lo:hi] + update
         return jnp.sum(wide * wide, axis=1, keepdims=True)
 
-    squares = take(tp)
+    squares = take(tp, True)
     got_tok(mate)
     squares = squares + take(mate)
     for k, x in enumerate(far):
@@ -118,7 +130,7 @@
     def project(ref, lo, hi):
         return (inv * dot(scaled[...], ref[:, lo:hi])).astype(BF16)
 
-    pre = inv * dot(scaled[...], vg[...], ((1,), (1,))) + raw_b[0:1, :]
+    pre = inv * acc_c[:, 2 * mem:2 * mem + GROUP] + raw_b[0:1, :]
     lf = jnp.minimum(pre, 0.0) - jnp.log1p(jnp.exp(-jnp.abs(pre)))
     row_id = lax.broadcasted_iota(jnp.int32, (count, count), 0)
     col_id = lax.broadcasted_iota(jnp.int32, (count, count), 1)
@@ -136,8 +148,6 @@
         top = jnp.max(decays, axis=1, keepdims=True)
         return i_col, b_col, decays, top
 
-    wait_of["k"].wait()
-    wait_of["v"].wait()
     scale = head_dim ** -0.5
     a_sends = []
 
@@ -147,8 +157,8 @@
 
     for h in range(heads):
         lo, hi = h * head_dim, (h + 1) * head_dim
-        ks[:, lo:hi] = project(vk, lo, hi)
-        vs[:, lo:hi] = project(vv, lo, hi)
+        ks[:, lo:hi] = (inv * acc_c[:, lo:hi]).astype(BF16)
+        vs[:, lo:hi] = (inv * acc_c[:, mem + lo:mem + hi]).astype(BF16)
         i_col, b_col, _, top = gate_parts(h)
         total = b_col[count - 1:count, :]
         m_own = top[count - 1:count, :]
@@ -175,16 +185,17 @@
     mixed[...] = mix
     edge = remote(mixed.at[pl.ds(count - EXTRA, EXTRA)], halo, h_s, h_r, (sp + 1, tp))
     pl.when(sp < n_sp - 1)(edge.start)
+
+    wait_of["b"].wait()
+    wait_of["o"].wait()
     wait_of["q"].wait()
-    for h in range(heads):
-        qs[:, h * head_dim:(h + 1) * head_dim] = project(vq, h * head_dim, (h + 1) * head_dim)
-    wait_of["b"].wait()
-    gb[...] = project(vb, 0, conv)
-    wait_of["o"].wait()
-    for h in range(heads):
-        og[:, h * head_dim:(h + 1) * head_dim] = project(vo, h * head_dim, (h + 1) * head_dim)
 
     def local_part():
+        for h in range(heads):
+            qs[:, h * head_dim:(h + 1) * head_dim] = project(vq, h * head_dim, (h + 1) * head_dim)
+        gb[...] = project(vb, 0, conv)
+        for h in range(heads):
+            og[:, h * head_dim:(h + 1) * head_dim] = project(vo, h * head_dim, (h + 1) * head_dim)
         for h in range(heads):
             lo, hi = h * head_dim, (h + 1) * head_dim
             _, _, decays, top = gate_parts(h)
@@ -192,21 +203,6 @@
             den[h] = jnp.broadcast_to(jnp.sum(scores, axis=1, keepdims=True), (count, GROUP))
             num[h] = dot(scores.astype(BF16), vs[:, lo:hi])
 
-        @pl.when(sp > 0)
-        def _():
-            edge.wait_recv()
-
-        @pl.when(sp == 0)
-        def _():
-            halo[...] = jnp.zeros(halo.shape, BF16)
-        pad[0:EXTRA, :] = halo[...].astype(F32)
-        pad[EXTRA:EXTRA + count, :] = mixed[...].astype(F32)
-        reach = taps.shape[0] - 1
-        tap = taps[...].astype(F32)
-        acc = tap[0:1, :] * pad[EXTRA - reach:EXTRA - reach + count, :]
-        for j in range(1, reach + 1):
-            acc = acc + tap[j:j + 1, :] * pad[EXTRA - reach + j:EXTRA - reach + j + count, :]
-        yc[...] = (gb[...].astype(F32) * acc).astype(BF16)
 
     early = pair >= (last_pair + 1) // 2
     pl.when(early)(local_part)
@@ -264,6 +260,23 @@
             in_c[h, at, :] = (f_p * block_p + f_e * block_a).astype(BF16)
 
     pl.when(jnp.logical_not(early))(local_part)
+
+    @pl.when(sp > 0)
+    def _():
+        edge.wait_recv()
+
+    @pl.when(sp == 0)
+    def _():
+        halo[...] = jnp.zeros(halo.shape, BF16)
+    pad[0:EXTRA, :] = halo[...].astype(F32)
+    pad[EXTRA:EXTRA + count, :] = mixed[...].astype(F32)
+    reach = taps.shape[0] - 1
+    tap = taps[...].astype(F32)
+    acc = tap[0:1, :] * pad[EXTRA - reach:EXTRA - reach + count, :]
+    for j in range(1, reach + 1):
+        acc = acc + tap[j:j + 1, :] * pad[EXTRA - reach + j:EXTRA - reach + j + count, :]
+    yc[...] = (gb[...].astype(F32) * acc).astype(BF16)
+
 
     own_sq = jnp.zeros((count, 1), F32)
     for h in range(heads):

time: 41.1 us -> 40.3 us (0.981)
  Pallas kernels: 39.3 us -> 38.5 us
    pallas_call x1, Pallas kernels: 39.3 us -> 38.5 us  [body(): pl.pallas_call(functools.partial(kernel, n_sp, n_tp, heads), out_shape=ja...]
where the time goes in v4:
time: 40.3 us; the launch traced here: 40.1 us
  Pallas kernels  38.5 us (96%)
  local copies, waits for them, and re-layouts  1.57 us (4%)
    pallas_call x1, Pallas kernels, body(): pl.pallas_call(functools.partial(kernel, n_sp, n_tp, heads), out_shape=ja...  38.5 us
    unnamed x1, local copies, waits for them, and re-layouts  1.57 us

profile of v4, /device:TPU:25, one launch (start us, length us, event | category | flops | bytes accessed | tf_op | source)
XLA Modules:
  0.0 40.1 jit_solution(12441327114304713336)
XLA Ops:
  0.0 38.5 %mixer.1 = bf16[32,2048]{1,0:T(8,128)(2,1)} custom-call(bf16[128,512]{1,0:T(8,128)(2,1)} %refs_0_.1, bf16[1,512]{1,0:T(2,128)(2,1)} %refs_1_.1, bf16[2048,256]{1,0:T(8,128)(2,1)} %refs_2_.1, bf16[2048,256]{1,0:T(8,128)(2,1)} %refs_3_.1, bf16[2048,256]{1,0:T(8,128)(2,1)} %refs_4_.1, bf16[3,256]{1,0:T(4,128)(2,1)} %refs_5_.1, bf16[2048,512]{1,0:T(8,128)(2,1)} %refs_6_.1, ...), custom_call_target="tpu_custom_call" | custom-call | tf_op jit(solution)/shard_map/mixer/pallas_call | solution.py:399
  38.5 1.6 %copy.17 = bf16[32,2048]{1,0:T(8,128)(2,1)} copy(bf16[32,2048]{1,0:T(8,128)(2,1)} %mixer.1) | data formatting | bytes 262144
